TPU v7x, 32 devices: a whole 2x2x4 slice. The times are simulated.
32 devices in a mesh: gr: 2 (over x), sp: 8 (over z, y), tp: 2 (over core).
Axes of the slice: x: 2, y: 2, z: 4, core: 2. Of those that a mesh axis runs over, the one named last changes fastest.
Arguments:
- prompt: bfloat16 [128, 128, 1024], P('gr', 'sp'), parts along dimension 0, may hold values from -6 to 6
- w_key: bfloat16 [1024, 8, 128], P(None, 'tp'), may hold values from -0.1875 to 0.1875
- w_value: bfloat16 [1024, 8, 128], P(None, 'tp'), may hold values from -0.1875 to 0.1875
- w_in_gate: bfloat16 [2, 1024, 8], P(None, None, 'tp'), may hold values from -0.1875 to 0.1875
- w_forget_gate: bfloat16 [2, 1024, 8], P(None, None, 'tp'), may hold values from -0.1875 to 0.1875
- in_bias: float32 [2, 8], P(None, 'tp'), may hold values from -6 to 0, as said below
- forget_bias: float32 [2, 8], P(None, 'tp'), may hold values from 1 to 10, as said below
- query: bfloat16 [128, 8, 128], P(('gr', 'sp'), 'tp'), parts along dimension 0, may hold values from -6 to 6
- w_out: bfloat16 [8, 128, 1024], P('tp'), may hold values from -0.5 to 0.5
Outputs:
- memory: bfloat16 [2, 128, 8, 128, 128], P(None, ('gr', 'sp'), 'tp'), parts along dimension 1
- normalizer: float32 [2, 128, 8, 128], P(None, ('gr', 'sp'), 'tp'), parts along dimension 1
- stabilizer: float32 [2, 128, 8], P(None, ('gr', 'sp'), 'tp'), parts along dimension 1
- read: bfloat16 [128, 1024], P(('gr', 'sp'), 'tp'), parts along dimension 0
There are 2 independent parts, one for each index of `gr`. A program takes and returns all parts, laid end to end along the dimension named above; an argument that names none is the same for every part. Nothing has to cross between parts.
Inputs may be any that keep to these rules, and one draw needn't show every extreme that they name: forget_bias lies between 1 and 10; the per-head share of memory kept over the whole prompt is spread between a few and some ninety percent. in_bias lies between -6 and 0.
All inputs are finite; a program needn't handle non-finite values.
Results may differ from a plain program's by a relative error of at most 0.015.
Values may be sent and summed in bfloat16 or wider, within the bound.
A program may use at most 64 MiB of HBM per device.

v0:
```python
import jax
import jax.numpy as jnp
from jax import lax
from jax.sharding import PartitionSpec as P

highest = lax.Precision.HIGHEST


def project(token_rows, w_key, w_value, w_in_gate, w_forget_gate, in_bias, forget_bias):
    key_rows = jnp.einsum(
        "bsd,dhe->bshe", token_rows, w_key, preferred_element_type=jnp.float32
    ).astype(jnp.bfloat16)
    value_rows = jnp.einsum(
        "bsd,dhe->bshe", token_rows, w_value, preferred_element_type=jnp.float32
    ).astype(jnp.bfloat16)
    in_pre = (
        jnp.einsum("bsd,gdh->bsgh", token_rows, w_in_gate, preferred_element_type=jnp.float32)
        + in_bias
    )
    forget_pre = (
        jnp.einsum("bsd,gdh->bsgh", token_rows, w_forget_gate, preferred_element_type=jnp.float32)
        + forget_bias
    )
    return (key_rows, value_rows, jnp.stack((in_pre, forget_pre), axis=2))


def summary(scaled, float_values, in_log, forget_log, backward):
    total_forget = jnp.sum(forget_log, axis=1)
    running = jnp.cumsum(forget_log, axis=1)
    if backward:
        log_weight = in_log + running - forget_log
    else:
        log_weight = in_log + total_forget[:, None, :] - running
    stable = jnp.maximum(total_forget, jnp.max(log_weight, axis=1))
    weight = jnp.exp(log_weight - stable[:, None, :])
    weighted = scaled * weight[..., None]
    memory = jnp.einsum("bshd,bshe->bhde", weighted, float_values, precision=highest)
    normal = jnp.sum(weighted, axis=1)
    return (memory, normal, stable)


def read_out(memory_bf, normal, stable, query_f):
    cells = memory_bf.astype(jnp.float32)
    numerator = jnp.sum(query_f[..., :, None] * cells, axis=-2)
    denominator = jnp.sum(query_f * normal, axis=-1)
    floor_value = jnp.maximum(jnp.maximum(jnp.abs(denominator), jnp.exp(-stable)), 1.0)
    return numerator / floor_value[..., None]


def body(prompt, w_key, w_value, w_in_gate, w_forget_gate, in_bias, forget_bias, query, w_out):
    token_rows = lax.all_to_all(prompt, "sp", split_axis=0, concat_axis=1, tiled=True)
    key_rows, value_rows, gate_values = project(
        token_rows, w_key, w_value, w_in_gate, w_forget_gate, in_bias, forget_bias
    )
    scaled = key_rows.astype(jnp.float32) * key_rows.shape[-1] ** (-0.5)
    float_values = value_rows.astype(jnp.float32)
    query_f = query.astype(jnp.float32)
    memories = []
    normals = []
    stables = []
    reads = []
    for course in range(2):
        memory, normal, stable = summary(
            scaled,
            float_values,
            gate_values[:, :, 0, course, :],
            jax.nn.log_sigmoid(gate_values[:, :, 1, course, :]),
            course == 1,
        )
        memory_bf = memory.astype(jnp.bfloat16)
        memories.append(memory_bf)
        normals.append(normal)
        stables.append(stable)
        reads.append(read_out(memory_bf, normal, stable, query_f))
    hidden = (reads[0] + reads[1]).astype(jnp.bfloat16)
    head_terms = jnp.einsum("bhd,hde->be", hidden, w_out, preferred_element_type=jnp.float32)
    read = lax.psum_scatter(head_terms, "tp", scatter_dimension=1, tiled=True).astype(jnp.bfloat16)
    return (jnp.stack(memories), jnp.stack(normals), jnp.stack(stables), read)


def solution(mesh):
    return jax.shard_map(
        body,
        mesh=mesh,
        in_specs=(
            P("gr", "sp", None),
            P(None, "tp", None),
            P(None, "tp", None),
            P(None, None, "tp"),
            P(None, None, "tp"),
            P(None, "tp"),
            P(None, "tp"),
            P(("gr", "sp"), "tp", None),
            P("tp", None, None),
        ),
        out_specs=(
            P(None, ("gr", "sp"), "tp", None, None),
            P(None, ("gr", "sp"), "tp", None),
            P(None, ("gr", "sp"), "tp"),
            P(("gr", "sp"), "tp"),
        ),
        check_vma=False,
    )
```

profile of v0, /device:TPU:0, one launch (start us, length us, event | category | flops | bytes accessed | tf_op | source)
XLA Modules:
  0.0 103.6 jit_solution(2272053196822618441)
XLA Ops:
  7.2 7.5 %all-to-all-start = ((bf16[64,16,1024]{2,1,0:T(8,128)(2,1)}), bf16[64,16,1024]{2,1,0:T(8,128)(2,1)S(1)}, u32[]{:S(2)}, u32[]{:S(2)}) async-start(bf16[64,16,1024]{2,1,0:T(8,128)(2,1)} %param.9), calls=%async_computation | async-start | bytes 4194304 | tf_op jit(solution)/shard_map/all_to_all | solution.py:51
  14.7 48.5 %all-to-all-done = bf16[64,16,1024]{2,1,0:T(8,128)(2,1)S(1)} async-done(((bf16[64,16,1024]{2,1,0:T(8,128)(2,1)}), bf16[64,16,1024]{2,1,0:T(8,128)(2,1)S(1)}, u32[]{:S(2)}, u32[]{:S(2)}) %all-to-all-start) | async-done | bytes 2097184 | tf_op jit(solution)/shard_map/all_to_all | solution.py:51
  63.2 1.3 %copy-done.1 = bf16[64,16,1024]{2,1,0:T(8,128)(2,1)} copy-done((bf16[64,16,1024]{2,1,0:T(8,128)(2,1)}, bf16[64,16,1024]{2,1,0:T(8,128)(2,1)S(1)}, u32[]{:S(2)}) %copy-start.1) | copy-done | bytes 2097176
  64.5 1.8 %copy.41 = bf16[8,8,16,1024]{3,2,0,1:T(8,128)(2,1)S(1)} copy(bf16[8,8,16,1024]{3,2,1,0:T(8,128)(2,1)} %bitcast.87) | data formatting | bytes 4194304 | tf_op jit(solution)/shard_map/all_to_all | solution.py:51
  66.4 0.6 fusion.20
  67.1 0.6 fusion.22
  67.7 0.1 fusion.12
  67.8 0.1 fusion.29
  67.9 0.1 copy.67
  68.0 0.1 copy.46
  68.1 1.0 copy.54
  69.1 2.0 %fusion.33 = f32[8,128,4]{2,0,1:T(8,128)} fusion(f32[8,128,4]{2,0,1:T(8,128)} %copy.54), kind=kOutput, calls=%fused_computation.60 | output fusion | flops 520192 | bytes 32768 | tf_op jit(solution)/shard_map/jit(cumsum)/reduce_window_sum | solution.py:29
  71.1 1.2 %copy.55 = f32[8,128,4]{1,0,2:T(8,128)S(1)} copy(f32[8,128,4]{2,0,1:T(8,128)} %fusion.33) | data formatting | bytes 32768 | tf_op jit(solution)/shard_map/jit(cumsum)/reduce_window_sum | solution.py:29
  72.3 1.0 %copy.47 = f32[8,128,4]{2,0,1:T(8,128)} copy(f32[8,128,4]{1,0,2:T(8,128)S(1)} %get-tuple-element.16) | data formatting | bytes 32768 | tf_op jit(solution)/shard_map/jit(log_sigmoid)/neg | solution.py:67
  73.4 2.0 %fusion.32 = f32[8,128,4]{2,0,1:T(8,128)} fusion(f32[8,128,4]{2,0,1:T(8,128)} %copy.47), kind=kOutput, calls=%fused_computation.59 | output fusion | flops 520192 | bytes 32768 | tf_op jit(solution)/shard_map/jit(cumsum)/reduce_window_sum | solution.py:29
  75.3 1.2 %copy.48 = f32[8,128,4]{1,0,2:T(8,128)S(1)} copy(f32[8,128,4]{2,0,1:T(8,128)} %fusion.32) | data formatting | bytes 32768 | tf_op jit(solution)/shard_map/jit(cumsum)/reduce_window_sum | solution.py:29
  76.5 0.2 fusion.30
  76.8 0.1 copy.50
  77.1 0.1 copy.58
  77.1 0.1 exponential_multiply_fusion.1
  77.3 2.6 %convolution_convert_fusion = bf16[8,128,4,128]{3,1,2,0:T(8,128)(2,1)S(1)} fusion(bf16[8,128,1024,1]{2,1,3,0:T(8,128)(2,1)S(1)} %bitcast.85, bf16[1024,4,128]{2,1,0:T(4,128)(2,1)} %param.11), kind=kOutput, calls=%fused_computation.11 | convolution fusion | flops 1074266112 | bytes 4194304 | tf_op jit(solution)/shard_map/bsd,dhe->bshe/dot_general | solution.py:13
  79.9 1.6 %fusion = (f32[8,4,128]{2,1,0:T(4,128)S(1)}, f32[8,4,128]{2,1,0:T(4,128)S(1)}, bf16[8,128,4,128]{3,1,2,0:T(8,128)(2,1)S(1)}) fusion(f32[8,128,4]{1,2,0:T(4,128)S(1)} %copy.51, f32[8,128,4]{1,2,0:T(4,128)S(1)} %copy.59, bf16[8,128,1024,1]{2,1,3,0:T(8,128)(2,1)S(1)} %bitcast.86, bf16[1024,4,128]{2,1,0:T(4,128)(2,1)S(1)} %copy-done.7), kind=kOutput, calls=%fused_computation.2 | convolution fusion | flops 1076879360 | bytes 4259840 | tf_op jit(solution)/shard_map/bsd,dhe->bshe/dot_general | solution.py:10
  81.5 0.1 multiply_reduce_fusion.3
  81.6 2.7 %fusion.4 = bf16[8,4,128,128]{3,2,1,0:T(8,128)(2,1)S(1)} fusion(bf16[8,128,4,128]{3,1,2,0:T(8,128)(2,1)S(1)} %convolution_convert_fusion, bf16[8,128,4,128]{3,1,2,0:T(8,128)(2,1)S(1)} %get-tuple-element.18, f32[8,128,4]{1,2,0:T(4,128)S(1)} %copy.59), kind=kOutput, calls=%fused_computation.9 | convolution fusion | flops 806879232 | bytes 3162112 | tf_op jit(solution)/shard_map/bshd,bshe->bhde/dot_general | solution.py:37
  84.3 3.3 %multiply_reduce_fusion.1 = (f32[8,4,128]{2,1,0:T(4,128)S(1)}, f32[8,4,128]{2,1,0:T(4,128)S(1)}, bf16[8,4,128,128]{3,2,1,0:T(8,128)(2,1)S(1)}) fusion(f32[8,4,128]{2,1,0:T(4,128)S(1)} %convert_element_type.36, bf16[8,4,128,128]{3,2,1,0:T(8,128)(2,1)S(1)} %fusion.4, bf16[8,128,4,128]{3,1,2,0:T(8,128)(2,1)S(1)} %convolution_convert_fusion, ...), kind=kOutput, calls=%fused_computation.8 | convolution fusion | flops 810016768 | bytes 4259840 | tf_op jit(solution)/shard_map/bshd,bshe->bhde/dot_general | solution.py:37
  87.6 0.1 fusion.24
  87.7 0.9 convolution_bitcast_fusion
  88.6 0.6 pad_maximum_fusion.1
  89.2 1.5 %pad_maximum_fusion = bf16[2,8,4,128,128]{4,3,2,1,0:T(8,128)(2,1)} fusion(bf16[1,8,4,128,128]{4,3,2,1,0:T(8,128)(2,1)S(1)} %bitcast.88, bf16[1,8,4,128,128]{4,3,2,1,0:T(8,128)(2,1)S(1)} %bitcast.89), kind=kLoop, calls=%fused_computation.6 | loop fusion | flops 1048576 | bytes 4194304 | tf_op jit(solution)/shard_map/stack | solution.py:78
  90.7 0.6 pad_maximum_fusion.2
  91.3 4.1 %reduce-scatter.2.cloned.1.call-done = f32[8,512]{1,0:T(8,128)} async-done(((f32[8,1024]{1,0:T(8,128)}), f32[8,512]{1,0:T(8,128)}) %reduce-scatter.2.cloned.1.call-update) | async-done | bytes 16400 | tf_op jit(solution)/shard_map/reduce_scatter | solution.py:77
  95.4 1.3 %convert_element_type.40 = bf16[8,512]{1,0:T(8,128)(2,1)} convert(f32[8,512]{1,0:T(8,128)} %reduce-scatter.2.cloned.1.call-done) | non-fusion elementwise | flops 4096 | bytes 24576 | tf_op jit(solution)/shard_map/convert_element_type | solution.py:77
  (28 shorter events, 0.4 us)
Async XLA Ops:
  7.2 80.6 %copy-start = (bf16[4,128,1024]{2,1,0:T(8,128)(2,1)S(1)}, bf16[4,128,1024]{2,1,0:T(8,128)(2,1)}, u32[]{:S(2)}) copy-start(bf16[4,128,1024]{2,1,0:T(8,128)(2,1)} %param.17) | copy-start | bytes 3145732
  7.2 7.5 %copy-start.2 = (bf16[8,4,128]{2,1,0:T(4,128)(2,1)S(1)}, bf16[8,4,128]{2,1,0:T(4,128)(2,1)}, u32[]{:S(2)}) copy-start(bf16[8,4,128]{2,1,0:T(4,128)(2,1)} %param.16) | copy-start | bytes 24580
  7.2 56.0 %all-to-all-start = ((bf16[64,16,1024]{2,1,0:T(8,128)(2,1)}), bf16[64,16,1024]{2,1,0:T(8,128)(2,1)S(1)}, u32[]{:S(2)}, u32[]{:S(2)}) async-start(bf16[64,16,1024]{2,1,0:T(8,128)(2,1)} %param.9), calls=%async_computation | async-start | bytes 4194304 | tf_op jit(solution)/shard_map/all_to_all | solution.py:51
  14.7 80.8 %reduce-scatter.2.cloned.1.call-start = ((), (), s32[]{:S(2)}) async-start(), calls=%async_computation.2 | async-start | bytes 49152 | tf_op jit(solution)/shard_map/reduce_scatter | solution.py:77
  63.2 1.3 %copy-start.1 = (bf16[64,16,1024]{2,1,0:T(8,128)(2,1)}, bf16[64,16,1024]{2,1,0:T(8,128)(2,1)S(1)}, u32[]{:S(2)}) copy-start(bf16[64,16,1024]{2,1,0:T(8,128)(2,1)S(1)} %all-to-all-done) | copy-start | bytes 6291460
  64.5 1.8 %copy-start.3 = (bf16[2,1024,4]{1,2,0:T(4,128)(2,1)S(1)}, bf16[2,1024,4]{1,2,0:T(4,128)(2,1)}, u32[]{:S(2)}) copy-start(bf16[2,1024,4]{1,2,0:T(4,128)(2,1)} %param.13) | copy-start | bytes 49156
  66.3 0.7 copy-start.4
  66.4 1.3 %copy-start.5 = (f32[2,4]{1,0:T(2,128)S(1)}, f32[2,4]{1,0:T(2,128)}, u32[]{:S(2)}) copy-start(f32[2,4]{1,0:T(2,128)} %param.15) | copy-start | bytes 100
  66.4 1.3 %copy-start.6 = (f32[2,4]{1,0:T(2,128)S(1)}, f32[2,4]{1,0:T(2,128)}, u32[]{:S(2)}) copy-start(f32[2,4]{1,0:T(2,128)} %param.14) | copy-start | bytes 100
  77.3 2.6 %copy-start.7 = (bf16[1024,4,128]{2,1,0:T(4,128)(2,1)S(1)}, bf16[1024,4,128]{2,1,0:T(4,128)(2,1)}, u32[]{:S(2)}) copy-start(bf16[1024,4,128]{2,1,0:T(4,128)(2,1)} %param.10) | copy-start | bytes 3145732
Sparse Core Ops, SparseCore 0:
  88.7 6.6 reduce-scatter.1
where the time goes:
time: 104 us
  waiting for transfers between devices  52.6 us (51%)
  between operations  14.2 us (14%)
  matrix products  12.3 us (12%)
  other arithmetic  8.64 us (8%)
  local copies, waits for them, and re-layouts  8.29 us (8%)
  starting transfers between devices  7.52 us (7%)
    all_to_all x1, waiting for transfers between devices, body(): lax.all_to_all(prompt, 'sp', split_axis=0, concat_axis=1, tiled=True)  48.5 us
    all_to_all x1, starting transfers between devices, body(): lax.all_to_all(prompt, 'sp', split_axis=0, concat_axis=1, tiled=True)  7.49 us
    dot_general x2, matrix products, summary(): jnp.einsum('bshd,bshe->bhde', weighted, float_values, precision=highest)  5.98 us
    reduce_scatter x1, waiting for transfers between devices, body(): lax.psum_scatter(head_terms, 'tp', scatter_dimension=1, tiled=True)  4.09 us
    another operation x2, other arithmetic, summary(): running = jnp.cumsum(forget_log, axis=1)  3.93 us
    another operation x3, other arithmetic, body(): return (jnp.stack(memories), jnp.stack(normals), jnp.stack(stables), read)  2.72 us
    dot_general x1, matrix products, project(): jnp.einsum('bsd,dhe->bshe', token_rows, w_value, preferred_element_type=j...  2.57 us
    another operation x2, local copies, waits for them, and re-layouts, summary(): running = jnp.cumsum(forget_log, axis=1)  2.45 us
  transfers between devices with their start and end apart: 2, of which 2 were waited for; matrix products, arithmetic and copies ran while one was open for 3% of the time, Pallas kernels for 0%

commit v1 on v0

v1 whole, which is shorter than its diff:
```python
import functools

import jax
import jax.numpy as jnp
from jax import lax
from jax.experimental import pallas as pl
from jax.experimental.pallas import tpu as pltpu
from jax.sharding import PartitionSpec as P

MESH = pl.DeviceIdType.MESH
F32 = jnp.float32
BF16 = jnp.bfloat16


def nt(a, b):
    return lax.dot_general(a, b, (((1,), (1,)), ((), ())), preferred_element_type=F32)


def kernel(
    n, tpn, heads, width, gates,
    prompt, wkt_hbm, wv_hbm, wo_hbm, bias, query,
    mem_out, norm_out, stab_out, read_out,
    xbuf, wkt, wv, wo, membuf, hid, stabs, parts, got,
    wsem, lsem, ssem, rsem, fsend, frecv, osem, xsend, xrecv,
):
    sp = lax.axis_index("sp")
    tp = lax.axis_index("tp")
    seqs, length, _ = xbuf.shape
    rounds = seqs // tpn
    block = length // n
    order = sorted(range(1, n), key=lambda k: abs(k - n / 2))

    barrier = pltpu.get_barrier_semaphore()
    for k in order:
        pl.semaphore_signal(
            barrier, inc=1, device_id={"sp": lax.rem(sp + k, n)}, device_id_type=MESH
        )
    for j in range(1, tpn):
        pl.semaphore_signal(
            barrier, inc=1, device_id={"tp": lax.rem(tp + j, tpn)}, device_id_type=MESH
        )

    weights = [
        pltpu.make_async_copy(wkt_hbm, wkt, wsem.at[0]),
        pltpu.make_async_copy(wv_hbm, wv, wsem.at[1]),
        pltpu.make_async_copy(wo_hbm, wo, wsem.at[2]),
    ]
    rows = pl.ds(pl.multiple_of(sp * block, block), block)

    def own(r):
        q = tp * rounds + r
        return pltpu.make_async_copy(prompt.at[sp * seqs + q], xbuf.at[q, rows], lsem.at[r])

    def send(r, k):
        q = tp * rounds + r
        dest = lax.rem(sp + k, n)
        return pltpu.make_async_remote_copy(
            src_ref=prompt.at[dest * seqs + q],
            dst_ref=xbuf.at[q, rows],
            send_sem=ssem.at[r, k],
            recv_sem=rsem.at[r, k],
            device_id={"sp": dest},
            device_id_type=MESH,
        )

    def forward(r, j):
        q = tp * rounds + r
        return pltpu.make_async_remote_copy(
            src_ref=xbuf.at[q],
            dst_ref=xbuf.at[q],
            send_sem=fsend.at[r, j],
            recv_sem=frecv.at[r, j],
            device_id={"tp": lax.rem(tp + j, tpn)},
            device_id_type=MESH,
        )

    def out(g, q):
        return pltpu.make_async_copy(membuf.at[g, q], mem_out.at[g, q], osem.at[g, q])

    pl.semaphore_wait(barrier, n - 1 + tpn - 1)
    for r in range(rounds):
        for k in order:
            send(r, k).start()
    for copy in weights:
        copy.start()
    for r in range(rounds):
        own(r).start()
    stabs[...] = jnp.zeros_like(stabs)
    for copy in weights:
        copy.wait()

    tri = (
        lax.broadcasted_iota(jnp.int32, (length, length), 0)
        <= lax.broadcasted_iota(jnp.int32, (length, length), 1)
    ).astype(F32)
    ahead = lax.broadcasted_iota(jnp.int32, (gates, length), 0) < heads
    lane = lax.broadcasted_iota(jnp.int32, (gates, stabs.shape[1]), 1)
    pick = lax.broadcasted_iota(jnp.int32, (16, length), 0)
    key_rows = heads * width

    def compute(q):
        x = xbuf[q]
        kt = nt(wkt[...], x)
        values = jnp.dot(x, wv[...], preferred_element_type=F32).astype(BF16)
        pre = kt[key_rows:] + bias[...]
        keys = kt[:key_rows].astype(BF16)
        in_log, forget_pre = pre[:gates], pre[gates:]
        forget = jnp.minimum(forget_pre, 0.0) - jnp.log1p(jnp.exp(-jnp.abs(forget_pre)))
        running = jnp.dot(
            forget, tri, preferred_element_type=F32, precision=lax.Precision.HIGHEST
        )
        total = jnp.sum(forget, axis=1, keepdims=True)
        log_weight = in_log + jnp.where(ahead, total - running, running - forget)
        stable = jnp.maximum(total, jnp.max(log_weight, axis=1, keepdims=True))
        weight = jnp.exp(log_weight - stable) * width ** (-0.5)
        floor = jnp.maximum(jnp.exp(-stable), 1.0)
        stabs[...] = jnp.where(lane == q, stable, stabs[...])
        high = weight.astype(BF16).astype(F32)
        split = jnp.concatenate([high, weight - high], axis=0).astype(BF16)
        queries = query[q]
        for h in range(heads):
            head = keys[h * width : (h + 1) * width]
            head_f = head.astype(F32)
            w0, w1 = weight[h : h + 1], weight[heads + h : heads + h + 1]
            scores = jnp.dot(queries, head, preferred_element_type=F32)[h : h + 1]
            q0, q1 = scores * w0, scores * w1
            both = jnp.where(lax.rem(pick, 2) == 0, q0, q1)
            top = both.astype(BF16).astype(F32)
            tail = jnp.where(pick < 2, top, jnp.where(pick < 4, both - top, 0.0)).astype(BF16)
            lhs = jnp.concatenate(
                [(head_f * w0).astype(BF16), (head_f * w1).astype(BF16), tail], axis=0
            )
            res = jnp.dot(
                lhs, values[:, h * width : (h + 1) * width], preferred_element_type=F32
            )
            membuf[0, q, h] = res[:width].astype(BF16)
            membuf[1, q, h] = res[width : 2 * width].astype(BF16)
            normal = nt(split, head)
            normal = normal[:gates] + normal[gates:]
            norm_out[0, q, h : h + 1] = normal[h : h + 1]
            norm_out[1, q, h : h + 1] = normal[heads + h : heads + h + 1]
            last = res[2 * width :]
            d0 = jnp.abs(jnp.sum(q0, axis=1, keepdims=True))
            d1 = jnp.abs(jnp.sum(q1, axis=1, keepdims=True))
            f0, f1 = floor[h : h + 1], floor[heads + h : heads + h + 1]
            hid[q, :, h * width : (h + 1) * width] = (
                (last[0:1] + last[2:3]) / jnp.maximum(d0, f0)
                + (last[1:2] + last[3:4]) / jnp.maximum(d1, f1)
            )
        for g in range(2):
            out(g, q).start()

    def turn(r, carry):
        own(r).wait()
        for k in order:
            send(r, k).wait_recv()
        for j in range(1, tpn):
            forward(r, j).start()
        compute(tp * rounds + r)
        for j in range(1, tpn):
            forward(r, j).wait_recv()
            compute(lax.rem(tp + tpn - j, tpn) * rounds + r)
        return carry

    lax.fori_loop(0, rounds, turn, 0)

    terms = jnp.dot(hid[:, 0, :].astype(BF16), wo[...], preferred_element_type=F32)
    share = terms.shape[1] // tpn
    for t in range(tpn):
        parts[t] = terms[:, t * share : (t + 1) * share]

    def give(j):
        peer = lax.rem(tp + j, tpn)
        return pltpu.make_async_remote_copy(
            src_ref=parts.at[peer],
            dst_ref=got.at[j],
            send_sem=xsend.at[j],
            recv_sem=xrecv.at[j],
            device_id={"tp": peer},
            device_id_type=MESH,
        )

    for j in range(1, tpn):
        give(j).start()
    turned = jnp.transpose(stabs[...])
    for g in range(2):
        stab_out[g] = turned[:seqs, g * heads : (g + 1) * heads]
    for r in range(rounds):
        for k in order:
            send(r, k).wait_send()
        for j in range(1, tpn):
            forward(r, j).wait_send()
    for g in range(2):
        for q in range(seqs):
            out(g, q).wait()
    total = parts[tp]
    for j in range(1, tpn):
        give(j).wait()
        total = total + got[j]
    read_out[...] = total.astype(BF16)


def solution(mesh):
    n, tpn = mesh.shape["sp"], mesh.shape["tp"]

    def body(prompt, w_key, w_value, w_in_gate, w_forget_gate, in_bias, forget_bias, query, w_out):
        depth, heads, width = w_key.shape
        seqs = prompt.shape[0] // n
        length = prompt.shape[1] * n
        rounds = seqs // tpn
        gates = -(-2 * heads // 8) * 8
        pad = gates - 2 * heads

        def gate_rows(w):
            return jnp.pad(w.transpose(0, 2, 1).reshape(2 * heads, depth), ((0, pad), (0, 0)))

        def bias_rows(b):
            return jnp.pad(b.reshape(2 * heads), (0, pad))

        wkt = jnp.concatenate(
            [
                w_key.transpose(1, 2, 0).reshape(heads * width, depth),
                gate_rows(w_in_gate),
                gate_rows(w_forget_gate),
            ]
        )
        wv = w_value.reshape(depth, heads * width)
        wo = w_out.reshape(heads * width, -1)
        bias = jnp.concatenate([bias_rows(in_bias), bias_rows(forget_bias)])[:, None]
        bias = jnp.broadcast_to(bias, (2 * gates, length))
        columns = wo.shape[1]
        any_ = pl.BlockSpec(memory_space=pl.ANY)
        vmem = pl.BlockSpec(memory_space=pltpu.VMEM)
        dma = pltpu.SemaphoreType.DMA
        return pl.pallas_call(
            functools.partial(kernel, n, tpn, heads, width, gates),
            out_shape=(
                jax.ShapeDtypeStruct((2, seqs, heads, width, width), BF16),
                jax.ShapeDtypeStruct((2, seqs, heads, width), F32),
                jax.ShapeDtypeStruct((2, seqs, heads), F32),
                jax.ShapeDtypeStruct((seqs, columns // tpn), BF16),
            ),
            in_specs=[any_, any_, any_, any_, vmem, vmem],
            out_specs=(any_, vmem, vmem, vmem),
            scratch_shapes=[
                pltpu.VMEM((seqs, length, depth), BF16),
                pltpu.VMEM(wkt.shape, BF16),
                pltpu.VMEM(wv.shape, BF16),
                pltpu.VMEM(wo.shape, BF16),
                pltpu.VMEM((2, seqs, heads, width, width), BF16),
                pltpu.VMEM((seqs, 1, heads * width), F32),
                pltpu.VMEM((gates, 128), F32),
                pltpu.VMEM((tpn, seqs, columns // tpn), F32),
                pltpu.VMEM((tpn, seqs, columns // tpn), F32),
                dma((3,)),
                dma((rounds,)),
                dma((rounds, n)),
                dma((rounds, n)),
                dma((rounds, tpn)),
                dma((rounds, tpn)),
                dma((2, seqs)),
                dma((tpn,)),
                dma((tpn,)),
            ],
            compiler_params=pltpu.CompilerParams(collective_id=0, has_side_effects=True),
            name="memories",
        )(prompt, wkt, wv, wo, bias, query)

    return jax.shard_map(
        body,
        mesh=mesh,
        in_specs=(
            P("gr", "sp", None),
            P(None, "tp", None),
            P(None, "tp", None),
            P(None, None, "tp"),
            P(None, None, "tp"),
            P(None, "tp"),
            P(None, "tp"),
            P(("gr", "sp"), "tp", None),
            P("tp", None, None),
        ),
        out_specs=(
            P(None, ("gr", "sp"), "tp", None, None),
            P(None, ("gr", "sp"), "tp", None),
            P(None, ("gr", "sp"), "tp"),
            P(("gr", "sp"), "tp"),
        ),
        check_vma=False,
    )
```

time: 104 us -> 50.4 us (0.48)
  waiting for transfers between devices: 52.6 us -> 0 us
  Pallas kernels: 0 us -> 35.7 us
  between operations: 14.2 us -> 0.66 us
  matrix products: 12.3 us -> 0 us
  starting transfers between devices: 7.52 us -> 0 us
  other arithmetic: 8.64 us -> 1.13 us
  local copies, waits for them, and re-layouts: 8.29 us -> 12.3 us
    all_to_all x1 -> x0, waiting for transfers between devices: 48.5 us -> none  [body(): lax.all_to_all(prompt, 'sp', split_axis=0, concat_axis=1, tiled=True)]
    pallas_call x0 -> x1, Pallas kernels: none -> 35.7 us  [body(): pl.pallas_call(functools.partial(kernel, n, tpn, heads, width, gates), ou...]
    dot_general x7 -> x0, matrix products: 12.3 us -> none  [the longest x2 5.98 us: summary(): jnp.einsum('bshd,bshe->bhde', weighted, float_values, precision=highest)]
    all_to_all x1 -> x0, starting transfers between devices: 7.49 us -> none  [body(): lax.all_to_all(prompt, 'sp', split_axis=0, concat_axis=1, tiled=True)]
    another operation x6 -> x0, other arithmetic: 6.73 us -> none  [the longest x2 3.93 us: summary(): running = jnp.cumsum(forget_log, axis=1)]
    reduce_scatter x1 -> x0, waiting for transfers between devices: 4.09 us -> none  [body(): lax.psum_scatter(head_terms, 'tp', scatter_dimension=1, tiled=True)]
    unnamed x20 -> x10, local copies, waits for them, and re-layouts: 1.72 us -> 5.57 us
    reshape x0 -> x4, local copies, waits for them, and re-layouts: none -> 2.97 us  [the longest x2 1.52 us: bias_rows(): return jnp.pad(b.reshape(2 * heads), (0, pad))]
  transfers between devices with their start and end apart: 2 -> 0, of which waited for: 2 -> 0; matrix products, arithmetic and copies ran while one was open for 3% -> 0% of each run, Pallas kernels for 0% -> 0%
where the time goes in v1:
time: 50.4 us; the launch traced here: 49.8 us
  Pallas kernels  35.7 us (71%)
  local copies, waits for them, and re-layouts  12.3 us (24%)
  other arithmetic  1.13 us (2%)
  between operations  0.66 us (1%)
    pallas_call x1, Pallas kernels, body(): pl.pallas_call(functools.partial(kernel, n, tpn, heads, width, gates), ou...  35.7 us
    unnamed x10, local copies, waits for them, and re-layouts  5.57 us
    transpose x1, local copies, waits for them, and re-layouts, body(): w_key.transpose(1, 2, 0).reshape(heads * width, depth)  1.7 us
    reshape x2, local copies, waits for them, and re-layouts, bias_rows(): return jnp.pad(b.reshape(2 * heads), (0, pad))  1.52 us
    reshape x2, local copies, waits for them, and re-layouts, gate_rows(): w.transpose(0, 2, 1).reshape(2 * heads, depth)  1.46 us
    pallas_call x1, local copies, waits for them, and re-layouts, body(): pl.pallas_call(functools.partial(kernel, n, tpn, heads, width, gates), ou...  1.37 us
    concatenate x1, other arithmetic, body(): jnp.concatenate([w_key.transpose(1, 2, 0).reshape(heads * width, depth),...  1.05 us

profile of v1, /device:TPU:0, one launch (start us, length us, event | category | flops | bytes accessed | tf_op | source)
XLA Modules:
  0.0 49.8 jit_solution(10434022027536659381)
XLA Ops:
  0.6 0.8 %reshape.35 = f32[8]{0:T(128)S(1)} reshape(f32[2,4]{1,0:T(2,128)} %param.14) | data formatting | bytes 64 | tf_op jit(solution)/shard_map/reshape | solution.py:218
  1.4 0.8 %reshape.36 = f32[8]{0:T(128)S(1)} reshape(f32[2,4]{1,0:T(2,128)} %param.15) | data formatting | bytes 64 | tf_op jit(solution)/shard_map/reshape | solution.py:218
  2.1 0.1 pad_maximum_fusion.1
  2.2 0.7 %broadcast_in_dim.2.bias = f32[16,128]{1,0:T(8,128)} broadcast(f32[16]{0:T(128)S(1)} %pad_maximum_fusion.1), dimensions={0} | broadcast | bytes 8256 | tf_op jit(solution)/shard_map/broadcast_in_dim | solution.py:230
  2.9 0.7 %reshape.31 = bf16[8,1024]{1,0:T(8,128)(2,1)S(1)} reshape(bf16[2,4,1024]{2,1,0:T(4,128)(2,1)} %bitcast.14) | data formatting | bytes 32768 | tf_op jit(solution)/shard_map/reshape | solution.py:215
  3.6 0.7 %reshape.32 = bf16[8,1024]{1,0:T(8,128)(2,1)S(1)} reshape(bf16[2,4,1024]{2,1,0:T(4,128)(2,1)} %bitcast.15) | data formatting | bytes 32768 | tf_op jit(solution)/shard_map/reshape | solution.py:215
  4.4 0.0 copy-start
  4.4 1.7 %copy.13 = bf16[4,128,1024]{2,1,0:T(8,128)(2,1)S(1)} copy(bf16[4,128,1024]{1,0,2:T(4,128)(2,1)} %bitcast.12) | data formatting | bytes 2097152 | tf_op jit(solution)/shard_map/transpose | solution.py:222
  6.1 1.1 %pad_maximum_fusion.wkt_hbm = bf16[528,1024]{1,0:T(8,128)(2,1)} fusion(bf16[8,1024]{1,0:T(8,128)(2,1)S(1)} %reshape.32, bf16[8,1024]{1,0:T(8,128)(2,1)S(1)} %reshape.31, bf16[512,1024]{1,0:T(8,128)(2,1)S(1)} %bitcast.10), kind=kLoop, calls=%fused_computation | loop fusion | flops 3244032 | bytes 2162688 | tf_op jit(solution)/shard_map/concatenate | solution.py:220
  7.1 0.0 copy-done
  7.1 1.2 %copy.17 = bf16[128,8,4,128]{3,1,2,0:T(8,128)(2,1)} copy(bf16[128,8,4,128]{3,2,1,0:T(4,128)(2,1)S(1)} %bitcast.13) | data formatting | bytes 2097152
  8.3 35.7 %memories.1 = (bf16[2,8,4,128,128]{4,3,2,1,0:T(8,128)(2,1)}, f32[2,8,4,128]{3,2,1,0:T(4,128)}, f32[2,8,4]{2,1,0:T(8,128)}, bf16[8,512]{1,0:T(8,128)(2,1)}) custom-call(bf16[64,16,1024]{2,1,0:T(8,128)(2,1)} %prompt.1, bf16[528,1024]{1,0:T(8,128)(2,1)} %pad_maximum_fusion.wkt_hbm, bf16[1024,512]{1,0:T(8,128)(2,1)} %bitcast.9, bf16[512,1024]{1,0:T(8,128)(2,1)} %bitcast.11, ...), custom_call_target="tpu_custom_call" | custom-call | tf_op jit(solution)/shard_map/memories/pallas_call | solution.py:235
  44.0 1.4 %copy.14 = f32[2,8,4]{1,2,0:T(4,128)} copy(f32[2,8,4]{2,1,0:T(8,128)} %get-tuple-element.6) | data formatting | bytes 512 | tf_op jit(solution)/shard_map/memories/pallas_call | solution.py:235
  45.4 0.0 copy-start.1
  45.4 0.0 copy-start.2
  45.4 3.2 %copy.21 = bf16[2,8,4,128,128]{4,3,2,1,0:T(8,128)(2,1)} copy(bf16[2,8,4,128,128]{4,3,2,1,0:T(8,128)(2,1)} %get-tuple-element.12) | data formatting | bytes 4194304
  48.5 0.0 copy-done.1
  48.5 0.6 %copy.22 = f32[2,8,4,128]{3,2,1,0:T(4,128)} copy(f32[2,8,4,128]{3,2,1,0:T(4,128)S(1)} %copy-done.1) | data formatting | bytes 65536
  49.2 0.0 copy-done.2
  49.2 0.6 %copy.23 = bf16[8,512]{1,0:T(8,128)(2,1)} copy(bf16[8,512]{1,0:T(8,128)(2,1)S(1)} %copy-done.2) | data formatting | bytes 16384
Async XLA Ops:
  4.4 2.8 %copy-start = (bf16[1024,4,128]{2,1,0:T(4,128)(2,1)S(1)}, bf16[1024,4,128]{2,1,0:T(4,128)(2,1)}, u32[]{:S(2)}) copy-start(bf16[1024,4,128]{2,1,0:T(4,128)(2,1)} %param.11) | copy-start | bytes 3145732
  45.4 3.2 %copy-start.1 = (f32[2,8,4,128]{3,2,1,0:T(4,128)S(1)}, f32[2,8,4,128]{3,2,1,0:T(4,128)}, u32[]{:S(2)}) copy-start(f32[2,8,4,128]{3,2,1,0:T(4,128)} %get-tuple-element.13) | copy-start | bytes 98308
  45.4 3.8 %copy-start.2 = (bf16[8,512]{1,0:T(8,128)(2,1)S(1)}, bf16[8,512]{1,0:T(8,128)(2,1)}, u32[]{:S(2)}) copy-start(bf16[8,512]{1,0:T(8,128)(2,1)} %get-tuple-element.15) | copy-start | bytes 24580

commit v2 on v1

--- a/solution.py
+++ b/solution.py
@@ -18,10 +18,10 @@
 
 def kernel(
     n, tpn, heads, width, gates,
-    prompt, wkt_hbm, wv_hbm, wo_hbm, bias, query,
-    mem_out, norm_out, stab_out, read_out,
-    xbuf, wkt, wv, wo, membuf, hid, stabs, parts, got,
-    wsem, lsem, ssem, rsem, fsend, frecv, osem, xsend, xrecv,
+    prompt, wk_hbm, wv_hbm, wo_hbm, in_gate, forget_gate, in_bias, forget_bias, query,
+    membuf, norm_out, stab_out, read_out,
+    xbuf, raw, wkt, wv, wo, bias, hid, stabs, parts, got,
+    wsem, lsem, ssem, rsem, fsend, frecv, xsend, xrecv,
 ):
     sp = lax.axis_index("sp")
     tp = lax.axis_index("tp")
@@ -41,8 +41,8 @@
         )
 
     weights = [
-        pltpu.make_async_copy(wkt_hbm, wkt, wsem.at[0]),
-        pltpu.make_async_copy(wv_hbm, wv, wsem.at[1]),
+        pltpu.make_async_copy(wk_hbm, raw.at[0], wsem.at[0]),
+        pltpu.make_async_copy(wv_hbm, raw.at[1], wsem.at[1]),
         pltpu.make_async_copy(wo_hbm, wo, wsem.at[2]),
     ]
     rows = pl.ds(pl.multiple_of(sp * block, block), block)
@@ -74,20 +74,38 @@
             device_id_type=MESH,
         )
 
-    def out(g, q):
-        return pltpu.make_async_copy(membuf.at[g, q], mem_out.at[g, q], osem.at[g, q])
-
+    for copy in weights:
+        copy.start()
+    for r in range(rounds):
+        own(r).start()
     pl.semaphore_wait(barrier, n - 1 + tpn - 1)
     for r in range(rounds):
         for k in order:
             send(r, k).start()
-    for copy in weights:
-        copy.start()
-    for r in range(rounds):
-        own(r).start()
     stabs[...] = jnp.zeros_like(stabs)
-    for copy in weights:
-        copy.wait()
+    key_rows = heads * width
+    depth = wv.shape[0]
+
+    def gate_rows(ref):
+        pieces = [ref[g].astype(F32) for g in range(2)]
+        if gates > 2 * heads:
+            pieces.append(jnp.zeros((gates - 2 * heads, depth), F32))
+        return jnp.concatenate(pieces, axis=0)
+
+    wkt[key_rows:] = jnp.concatenate([gate_rows(in_gate), gate_rows(forget_gate)], axis=0).astype(BF16)
+    line = lax.broadcasted_iota(jnp.int32, bias.shape, 0)
+    column = jnp.zeros(bias.shape, F32)
+    for base, ref in ((0, in_bias), (gates, forget_bias)):
+        for g in range(2):
+            for h in range(heads):
+                column = jnp.where(line == base + g * heads + h, ref[g, h], column)
+    bias[...] = column
+    weights[0].wait()
+    for d in range(0, depth, 128):
+        wkt[:key_rows, d : d + 128] = raw[0, d : d + 128].reshape(128, key_rows).T
+    weights[1].wait()
+    wv[...] = raw[1].reshape(depth, key_rows)
+    weights[2].wait()
 
     tri = (
         lax.broadcasted_iota(jnp.int32, (length, length), 0)
@@ -96,7 +114,6 @@
     ahead = lax.broadcasted_iota(jnp.int32, (gates, length), 0) < heads
     lane = lax.broadcasted_iota(jnp.int32, (gates, stabs.shape[1]), 1)
     pick = lax.broadcasted_iota(jnp.int32, (16, length), 0)
-    key_rows = heads * width
 
     def compute(q):
         x = xbuf[q]
@@ -147,8 +164,6 @@
                 (last[0:1] + last[2:3]) / jnp.maximum(d0, f0)
                 + (last[1:2] + last[3:4]) / jnp.maximum(d1, f1)
             )
-        for g in range(2):
-            out(g, q).start()
 
     def turn(r, carry):
         own(r).wait()
@@ -182,22 +197,29 @@
 
     for j in range(1, tpn):
         give(j).start()
-    turned = jnp.transpose(stabs[...])
     for g in range(2):
-        stab_out[g] = turned[:seqs, g * heads : (g + 1) * heads]
+        stab_out[g] = stabs[g * heads : (g + 1) * heads, :seqs]
     for r in range(rounds):
         for k in order:
             send(r, k).wait_send()
         for j in range(1, tpn):
             forward(r, j).wait_send()
-    for g in range(2):
-        for q in range(seqs):
-            out(g, q).wait()
     total = parts[tp]
     for j in range(1, tpn):
         give(j).wait()
         total = total + got[j]
     read_out[...] = total.astype(BF16)
+
+
+def publish(count, *refs):
+    sources, targets, sems = refs[:count], refs[count : 2 * count], refs[2 * count]
+    copies = [
+        pltpu.make_async_copy(a, b, sems.at[i]) for i, (a, b) in enumerate(zip(sources, targets))
+    ]
+    for copy in copies:
+        copy.start()
+    for copy in copies:
+        copy.wait()
 
 
 def solution(mesh):
@@ -209,45 +231,30 @@
         length = prompt.shape[1] * n
         rounds = seqs // tpn
         gates = -(-2 * heads // 8) * 8
-        pad = gates - 2 * heads
-
-        def gate_rows(w):
-            return jnp.pad(w.transpose(0, 2, 1).reshape(2 * heads, depth), ((0, pad), (0, 0)))
-
-        def bias_rows(b):
-            return jnp.pad(b.reshape(2 * heads), (0, pad))
-
-        wkt = jnp.concatenate(
-            [
-                w_key.transpose(1, 2, 0).reshape(heads * width, depth),
-                gate_rows(w_in_gate),
-                gate_rows(w_forget_gate),
-            ]
-        )
-        wv = w_value.reshape(depth, heads * width)
         wo = w_out.reshape(heads * width, -1)
-        bias = jnp.concatenate([bias_rows(in_bias), bias_rows(forget_bias)])[:, None]
-        bias = jnp.broadcast_to(bias, (2 * gates, length))
         columns = wo.shape[1]
         any_ = pl.BlockSpec(memory_space=pl.ANY)
         vmem = pl.BlockSpec(memory_space=pltpu.VMEM)
+        smem = pl.BlockSpec(memory_space=pltpu.SMEM)
         dma = pltpu.SemaphoreType.DMA
-        return pl.pallas_call(
+        shapes = (
+            ((2, seqs, heads, width, width), BF16),
+            ((2, seqs, heads, width), F32),
+            ((2, heads, seqs), F32),
+            ((seqs, columns // tpn), BF16),
+        )
+        held = pl.pallas_call(
             functools.partial(kernel, n, tpn, heads, width, gates),
-            out_shape=(
-                jax.ShapeDtypeStruct((2, seqs, heads, width, width), BF16),
-                jax.ShapeDtypeStruct((2, seqs, heads, width), F32),
-                jax.ShapeDtypeStruct((2, seqs, heads), F32),
-                jax.ShapeDtypeStruct((seqs, columns // tpn), BF16),
-            ),
-            in_specs=[any_, any_, any_, any_, vmem, vmem],
-            out_specs=(any_, vmem, vmem, vmem),
+            out_shape=tuple(pltpu.VMEM(*shape) for shape in shapes),
+            in_specs=[any_] * 4 + [vmem, vmem, smem, smem, vmem],
+            out_specs=(vmem,) * 4,
             scratch_shapes=[
                 pltpu.VMEM((seqs, length, depth), BF16),
-                pltpu.VMEM(wkt.shape, BF16),
-                pltpu.VMEM(wv.shape, BF16),
+                pltpu.VMEM((2, depth, heads, width), BF16),
+                pltpu.VMEM((heads * width + 2 * gates, depth), BF16),
+                pltpu.VMEM((depth, heads * width), BF16),
                 pltpu.VMEM(wo.shape, BF16),
-                pltpu.VMEM((2, seqs, heads, width, width), BF16),
+                pltpu.VMEM((2 * gates, length), F32),
                 pltpu.VMEM((seqs, 1, heads * width), F32),
                 pltpu.VMEM((gates, 128), F32),
                 pltpu.VMEM((tpn, seqs, columns // tpn), F32),
@@ -258,13 +265,25 @@
                 dma((rounds, n)),
                 dma((rounds, tpn)),
                 dma((rounds, tpn)),
-                dma((2, seqs)),
                 dma((tpn,)),
                 dma((tpn,)),
             ],
             compiler_params=pltpu.CompilerParams(collective_id=0, has_side_effects=True),
             name="memories",
-        )(prompt, wkt, wv, wo, bias, query)
+        )(
+            prompt, w_key, w_value, wo,
+            w_in_gate.transpose(0, 2, 1), w_forget_gate.transpose(0, 2, 1),
+            in_bias, forget_bias, query,
+        )
+        memory, normal, stable, read = pl.pallas_call(
+            functools.partial(publish, len(shapes)),
+            out_shape=tuple(jax.ShapeDtypeStruct(*shape) for shape in shapes),
+            in_specs=[vmem] * len(shapes),
+            out_specs=(any_,) * len(shapes),
+            scratch_shapes=[dma((len(shapes),))],
+            name="outputs",
+        )(*[pltpu.with_memory_space_constraint(a, pltpu.VMEM) for a in held])
+        return memory, normal, stable.transpose(0, 2, 1), read
 
     return jax.shard_map(
         body,

time: 50.4 us -> 37.6 us (0.75)
  local copies, waits for them, and re-layouts: 12.3 us -> 0 us
  other arithmetic: 1.13 us -> 0 us
  Pallas kernels: 35.7 us -> 36.7 us
    unnamed x10 -> x0, local copies, waits for them, and re-layouts: 5.57 us -> none
    reshape x4 -> x0, local copies, waits for them, and re-layouts: 2.97 us -> none  [the longest x2 1.52 us: bias_rows(): return jnp.pad(b.reshape(2 * heads), (0, pad))]
    transpose x1 -> x0, local copies, waits for them, and re-layouts: 1.7 us -> none  [body(): w_key.transpose(1, 2, 0).reshape(heads * width, depth)]
    pallas_call x1 -> x0, local copies, waits for them, and re-layouts: 1.37 us -> none  [body(): pl.pallas_call(functools.partial(kernel, n, tpn, heads, width, gates), ou...]
    pallas_call x0 -> x1, Pallas kernels: none -> 1.36 us  [body(): pl.pallas_call(functools.partial(publish, len(shapes)), out_shape=tuple((...]
    concatenate x2 -> x0, other arithmetic: 1.13 us -> none  [the longest x1 1.05 us: body(): jnp.concatenate([w_key.transpose(1, 2, 0).reshape(heads * width, depth),...]
    broadcast_in_dim x1 -> x0, local copies, waits for them, and re-layouts: 0.67 us -> none  [body(): bias = jnp.broadcast_to(bias, (2 * gates, length))]
where the time goes in v2:
time: 37.6 us; the launch traced here: 37.3 us
  Pallas kernels  36.7 us (98%)
  between operations  0.64 us (2%)
    pallas_call x1, Pallas kernels, body(): pl.pallas_call(functools.partial(kernel, n, tpn, heads, width, gates), ou...  35.3 us
    pallas_call x1, Pallas kernels, body(): pl.pallas_call(functools.partial(publish, len(shapes)), out_shape=tuple((...  1.36 us

profile of v2, /device:TPU:0, one launch (start us, length us, event | category | flops | bytes accessed | tf_op | source)
XLA Modules:
  0.0 37.3 jit_solution(2823505022342081390)
XLA Ops:
  0.6 35.3 %memories.1 = (bf16[2,8,4,128,128]{4,3,2,1,0:T(8,128)(2,1)S(1)}, f32[2,8,4,128]{3,2,1,0:T(4,128)S(1)}, f32[2,4,8]{2,1,0:T(4,128)S(1)}, bf16[8,512]{1,0:T(8,128)(2,1)S(1)}) custom-call(bf16[64,16,1024]{2,1,0:T(8,128)(2,1)} %prompt.1, bf16[1024,4,128]{2,1,0:T(4,128)(2,1)} %wk_hbm.1, bf16[1024,4,128]{2,1,0:T(4,128)(2,1)} %wv_hbm.1, bf16[512,1024]{1,0:T(8,128)(2,1)} %bitcast.4, ...), custom_call_target="tpu_custom_call" | custom-call | tf_op jit(solution)/shard_map/memories/pallas_call | solution.py:246
  36.0 1.4 %outputs.1 = (bf16[2,8,4,128,128]{4,3,2,1,0:T(8,128)(2,1)}, f32[2,8,4,128]{3,2,1,0:T(4,128)}, f32[2,4,8]{2,1,0:T(4,128)}, bf16[8,512]{1,0:T(8,128)(2,1)}) custom-call(bf16[2,8,4,128,128]{4,3,2,1,0:T(8,128)(2,1)S(1)} %get-tuple-element.12.refs_0_, f32[2,8,4,128]{3,2,1,0:T(4,128)S(1)} %get-tuple-element.13.refs_1_, f32[2,4,8]{2,1,0:T(4,128)S(1)} %get-tuple-element.14.refs_2_, ...), custom_call_target="tpu_custom_call" | custom-call | tf_op jit(solution)/shard_map/outputs/pallas_call | solution.py:278

commit v3 on v2

--- a/solution.py
+++ b/solution.py
@@ -18,9 +18,9 @@
 
 def kernel(
     n, tpn, heads, width, gates,
-    prompt, wk_hbm, wv_hbm, wo_hbm, in_gate, forget_gate, in_bias, forget_bias, query,
+    prompt, wk_hbm, wv_hbm, wo_hbm, ig_hbm, fg_hbm, ib_hbm, fb_hbm, q_hbm,
     membuf, norm_out, stab_out, read_out,
-    xbuf, raw, wkt, wv, wo, bias, hid, stabs, parts, got,
+    in_gate, forget_gate, in_bias, forget_bias, query, xbuf, raw, wkt, wv, wo, bias, hid, stabs, parts, got,
     wsem, lsem, ssem, rsem, fsend, frecv, xsend, xrecv,
 ):
     sp = lax.axis_index("sp")
@@ -44,6 +44,11 @@
         pltpu.make_async_copy(wk_hbm, raw.at[0], wsem.at[0]),
         pltpu.make_async_copy(wv_hbm, raw.at[1], wsem.at[1]),
         pltpu.make_async_copy(wo_hbm, wo, wsem.at[2]),
+        pltpu.make_async_copy(ig_hbm, in_gate, wsem.at[3]),
+        pltpu.make_async_copy(fg_hbm, forget_gate, wsem.at[4]),
+        pltpu.make_async_copy(ib_hbm, in_bias, wsem.at[5]),
+        pltpu.make_async_copy(fb_hbm, forget_bias, wsem.at[6]),
+        pltpu.make_async_copy(q_hbm, query, wsem.at[7]),
     ]
     rows = pl.ds(pl.multiple_of(sp * block, block), block)
 
@@ -83,6 +88,8 @@
         for k in order:
             send(r, k).start()
     stabs[...] = jnp.zeros_like(stabs)
+    for copy in weights[3:]:
+        copy.wait()
     key_rows = heads * width
     depth = wv.shape[0]
 
@@ -98,7 +105,9 @@
     for base, ref in ((0, in_bias), (gates, forget_bias)):
         for g in range(2):
             for h in range(heads):
-                column = jnp.where(line == base + g * heads + h, ref[g, h], column)
+                column = jnp.where(
+                    line == base + g * heads + h, ref[g : g + 1, h : h + 1], column
+                )
     bias[...] = column
     weights[0].wait()
     for d in range(0, depth, 128):
@@ -110,7 +119,7 @@
     tri = (
         lax.broadcasted_iota(jnp.int32, (length, length), 0)
         <= lax.broadcasted_iota(jnp.int32, (length, length), 1)
-    ).astype(F32)
+    ).astype(BF16)
     ahead = lax.broadcasted_iota(jnp.int32, (gates, length), 0) < heads
     lane = lax.broadcasted_iota(jnp.int32, (gates, stabs.shape[1]), 1)
     pick = lax.broadcasted_iota(jnp.int32, (16, length), 0)
@@ -123,10 +132,13 @@
         keys = kt[:key_rows].astype(BF16)
         in_log, forget_pre = pre[:gates], pre[gates:]
         forget = jnp.minimum(forget_pre, 0.0) - jnp.log1p(jnp.exp(-jnp.abs(forget_pre)))
-        running = jnp.dot(
-            forget, tri, preferred_element_type=F32, precision=lax.Precision.HIGHEST
-        )
-        total = jnp.sum(forget, axis=1, keepdims=True)
+        first = forget.astype(BF16).astype(F32)
+        second = (forget - first).astype(BF16).astype(F32)
+        third = forget - first - second
+        pieces = jnp.concatenate([first, second, third, jnp.zeros_like(third)], axis=0)
+        sums = jnp.dot(pieces.astype(BF16), tri, preferred_element_type=F32)
+        running = sums[:gates] + sums[gates : 2 * gates] + sums[2 * gates : 3 * gates]
+        total = running[:, length - 1 :]
         log_weight = in_log + jnp.where(ahead, total - running, running - forget)
         stable = jnp.maximum(total, jnp.max(log_weight, axis=1, keepdims=True))
         weight = jnp.exp(log_weight - stable) * width ** (-0.5)
@@ -235,7 +247,6 @@
         columns = wo.shape[1]
         any_ = pl.BlockSpec(memory_space=pl.ANY)
         vmem = pl.BlockSpec(memory_space=pltpu.VMEM)
-        smem = pl.BlockSpec(memory_space=pltpu.SMEM)
         dma = pltpu.SemaphoreType.DMA
         shapes = (
             ((2, seqs, heads, width, width), BF16),
@@ -246,9 +257,14 @@
         held = pl.pallas_call(
             functools.partial(kernel, n, tpn, heads, width, gates),
             out_shape=tuple(pltpu.VMEM(*shape) for shape in shapes),
-            in_specs=[any_] * 4 + [vmem, vmem, smem, smem, vmem],
+            in_specs=[any_] * 9,
             out_specs=(vmem,) * 4,
             scratch_shapes=[
+                pltpu.VMEM((2, heads, depth), BF16),
+                pltpu.VMEM((2, heads, depth), BF16),
+                pltpu.VMEM((2, heads), F32),
+                pltpu.VMEM((2, heads), F32),
+                pltpu.VMEM((seqs, heads, width), BF16),
                 pltpu.VMEM((seqs, length, depth), BF16),
                 pltpu.VMEM((2, depth, heads, width), BF16),
                 pltpu.VMEM((heads * width + 2 * gates, depth), BF16),
@@ -259,7 +275,7 @@
                 pltpu.VMEM((gates, 128), F32),
                 pltpu.VMEM((tpn, seqs, columns // tpn), F32),
                 pltpu.VMEM((tpn, seqs, columns // tpn), F32),
-                dma((3,)),
+                dma((8,)),
                 dma((rounds,)),
                 dma((rounds, n)),
                 dma((rounds, n)),

time: 37.6 us -> 37.2 us (0.989)
  Pallas kernels: 36.7 us -> 36.2 us
    pallas_call x1, Pallas kernels: 35.3 us -> 34.9 us  [body(): pl.pallas_call(functools.partial(kernel, n, tpn, heads, width, gates), ou...]
where the time goes in v3:
time: 37.2 us; the launch traced here: 36.9 us
  Pallas kernels  36.2 us (97%)
  between operations  0.64 us (2%)
    pallas_call x1, Pallas kernels, body(): pl.pallas_call(functools.partial(kernel, n, tpn, heads, width, gates), ou...  34.9 us
    pallas_call x1, Pallas kernels, body(): pl.pallas_call(functools.partial(publish, len(shapes)), out_shape=tuple((...  1.36 us

profile of v3, /device:TPU:0, one launch (start us, length us, event | category | flops | bytes accessed | tf_op | source)
XLA Modules:
  0.0 36.9 jit_solution(3999189772736133124)
XLA Ops:
  0.6 34.9 %memories.1 = (bf16[2,8,4,128,128]{4,3,2,1,0:T(8,128)(2,1)S(1)}, f32[2,8,4,128]{3,2,1,0:T(4,128)S(1)}, f32[2,4,8]{2,1,0:T(4,128)S(1)}, bf16[8,512]{1,0:T(8,128)(2,1)S(1)}) custom-call(bf16[64,16,1024]{2,1,0:T(8,128)(2,1)} %prompt.1, bf16[1024,4,128]{2,1,0:T(4,128)(2,1)} %wk_hbm.1, bf16[1024,4,128]{2,1,0:T(4,128)(2,1)} %wv_hbm.1, bf16[512,1024]{1,0:T(8,128)(2,1)} %bitcast.4, ...), custom_call_target="tpu_custom_call" | custom-call | tf_op jit(solution)/shard_map/memories/pallas_call | solution.py:257
  35.5 1.4 %outputs.1 = (bf16[2,8,4,128,128]{4,3,2,1,0:T(8,128)(2,1)}, f32[2,8,4,128]{3,2,1,0:T(4,128)}, f32[2,4,8]{2,1,0:T(4,128)}, bf16[8,512]{1,0:T(8,128)(2,1)}) custom-call(bf16[2,8,4,128,128]{4,3,2,1,0:T(8,128)(2,1)S(1)} %get-tuple-element.12.refs_0_, f32[2,8,4,128]{3,2,1,0:T(4,128)S(1)} %get-tuple-element.13.refs_1_, f32[2,4,8]{2,1,0:T(4,128)S(1)} %get-tuple-element.14.refs_2_, ...), custom_call_target="tpu_custom_call" | custom-call | tf_op jit(solution)/shard_map/outputs/pallas_call | solution.py:294

commit v4 on v3

--- a/solution.py
+++ b/solution.py
@@ -124,10 +124,12 @@
     lane = lax.broadcasted_iota(jnp.int32, (gates, stabs.shape[1]), 1)
     pick = lax.broadcasted_iota(jnp.int32, (16, length), 0)
 
-    def compute(q):
+    def project(q):
         x = xbuf[q]
-        kt = nt(wkt[...], x)
         values = jnp.dot(x, wv[...], preferred_element_type=F32).astype(BF16)
+        return nt(wkt[...], x), values
+
+    def compute(q, kt, values):
         pre = kt[key_rows:] + bias[...]
         keys = kt[:key_rows].astype(BF16)
         in_log, forget_pre = pre[:gates], pre[gates:]
@@ -183,10 +185,14 @@
             send(r, k).wait_recv()
         for j in range(1, tpn):
             forward(r, j).start()
-        compute(tp * rounds + r)
+        before = (tp * rounds + r, *project(tp * rounds + r))
         for j in range(1, tpn):
             forward(r, j).wait_recv()
-            compute(lax.rem(tp + tpn - j, tpn) * rounds + r)
+            q = lax.rem(tp + tpn - j, tpn) * rounds + r
+            after = (q, *project(q))
+            compute(*before)
+            before = after
+        compute(*before)
         return carry
 
     lax.fori_loop(0, rounds, turn, 0)

time: 37.2 us -> 36.7 us (0.987)
  no operation moved by 1% of the time
where the time goes in v4:
time: 36.7 us; the launch traced here: 36.5 us
  Pallas kernels  35.9 us (98%)
  between operations  0.64 us (2%)
    pallas_call x1, Pallas kernels, body(): pl.pallas_call(functools.partial(kernel, n, tpn, heads, width, gates), ou...  34.5 us
    pallas_call x1, Pallas kernels, body(): pl.pallas_call(functools.partial(publish, len(shapes)), out_shape=tuple((...  1.36 us

profile of v4, /device:TPU:0, one launch (start us, length us, event | category | flops | bytes accessed | tf_op | source)
XLA Modules:
  0.0 36.5 jit_solution(1099212953260153153)
XLA Ops:
  0.6 34.5 %memories.1 = (bf16[2,8,4,128,128]{4,3,2,1,0:T(8,128)(2,1)S(1)}, f32[2,8,4,128]{3,2,1,0:T(4,128)S(1)}, f32[2,4,8]{2,1,0:T(4,128)S(1)}, bf16[8,512]{1,0:T(8,128)(2,1)S(1)}) custom-call(bf16[64,16,1024]{2,1,0:T(8,128)(2,1)} %prompt.1, bf16[1024,4,128]{2,1,0:T(4,128)(2,1)} %wk_hbm.1, bf16[1024,4,128]{2,1,0:T(4,128)(2,1)} %wv_hbm.1, bf16[512,1024]{1,0:T(8,128)(2,1)} %bitcast.4, ...), custom_call_target="tpu_custom_call" | custom-call | tf_op jit(solution)/shard_map/memories/pallas_call | solution.py:263
  35.2 1.4 %outputs.1 = (bf16[2,8,4,128,128]{4,3,2,1,0:T(8,128)(2,1)}, f32[2,8,4,128]{3,2,1,0:T(4,128)}, f32[2,4,8]{2,1,0:T(4,128)}, bf16[8,512]{1,0:T(8,128)(2,1)}) custom-call(bf16[2,8,4,128,128]{4,3,2,1,0:T(8,128)(2,1)S(1)} %get-tuple-element.12.refs_0_, f32[2,8,4,128]{3,2,1,0:T(4,128)S(1)} %get-tuple-element.13.refs_1_, f32[2,4,8]{2,1,0:T(4,128)S(1)} %get-tuple-element.14.refs_2_, ...), custom_call_target="tpu_custom_call" | custom-call | tf_op jit(solution)/shard_map/outputs/pallas_call | solution.py:300
